TPU v7x, 512 devices: a whole 4x4x16 slice. The times are simulated.
512 devices in a mesh: sp: 64 (over z, y), tp: 8 (over x, core).
Axes of the slice: x: 4, y: 4, z: 16, core: 2. Of those that a mesh axis runs over, the one named last changes fastest.
Arguments:
- tokens: bfloat16 [6144, 4, 1024], P(('sp', 'tp')), may hold values from -6 to 6
- in_gain: float32 [1024], replicated, may hold values from 0.1 to 1.9
- w_query: bfloat16 [1024, 1024], P('sp', 'tp'), may hold values from -0.1875 to 0.1875
- w_key: bfloat16 [1024, 1024], P('sp', 'tp'), may hold values from -0.1875 to 0.1875
- w_value: bfloat16 [1024, 1024], P('sp', 'tp'), may hold values from -0.1875 to 0.1875
- w_gate: bfloat16 [1024, 1024], P('sp', 'tp'), may hold values from -0.1875 to 0.1875
- w_beta: bfloat16 [1024, 8], P('sp', 'tp'), may hold values from -0.1875 to 0.1875
- conv_query: bfloat16 [4, 1024], P(None, 'tp'), may hold values from -3 to 3
- conv_key: bfloat16 [4, 1024], P(None, 'tp'), may hold values from -3 to 3
- conv_value: bfloat16 [4, 1024], P(None, 'tp'), may hold values from -3 to 3
- decay_rate: float32 [8], P('tp'), may hold values from 0.1 to 3
- out_gain: float32 [128], replicated, may hold values from 0.1 to 1.9
- w_out: bfloat16 [1024, 1024], P('tp', 'sp'), may hold values from -0.1875 to 0.1875
Outputs:
- mixed: bfloat16 [6144, 4, 1024], P(('sp', 'tp'))
All inputs are finite; a program needn't handle non-finite values.
Results may differ from a plain program's by a relative error of at most 0.02.
Values may be sent and summed in bfloat16 or wider, within the bound.
A program may use at most 64 MiB of HBM per device.

v0:
```python
import math

import jax
import jax.numpy as jnp
from jax import lax
from jax.sharding import Mesh
from jax.sharding import PartitionSpec as P

BLOCK = 32
SP = ("sp_0", "sp_1")
TP = ("tp_0", "tp_1")
SP_TP = ("sp_0", "sp_1", "tp_0", "tp_1")


epsilon = 1e-06
out_epsilon = 1e-10
highest = lax.Precision.DEFAULT


def in_order(pieces, dim):
    pieces = jnp.moveaxis(pieces, 0, dim)
    dims = pieces.shape
    return pieces.reshape(*dims[:dim], dims[dim] * dims[dim + 1], *dims[dim + 2 :])


def one_gather(arrays, axis, dims):
    flat = jnp.concatenate([a.reshape(-1) for a in arrays])
    lines, at, done = lax.all_gather(flat, axis), 0, []
    for a, dim in zip(arrays, dims):
        pieces = lines[:, at : at + a.size].reshape(-1, *a.shape)
        done.append(in_order(pieces, dim))
        at += a.size
    return tuple(done)


def gather_axes(x, axes, dim):
    filled = x
    for number in range(len(axes) - 1, -1, -1):
        filled = lax.all_gather(filled, axes[number], axis=dim, tiled=True)
    return filled


def cut_rows(length, count):
    unit = 8 if length >= 8 * count else 1
    return [length // unit * k // count * unit for k in range(1, count)]


def all_blocks(x, axes, sequence):
    pieces = x
    for k in sequence:
        pieces = lax.all_gather(pieces, axes[k])
    done = sequence[::-1]
    back = [done.index(k) for k in range(len(axes))]
    pieces = pieces.transpose(*back, *range(len(axes), pieces.ndim))
    return pieces.reshape(-1, *x.shape)


def gather_at_once(x, axes, dim):
    cut = max(range(max(1, x.ndim - 1)), key=lambda d: x.shape[d])
    count, done = len(axes), []
    for leading, piece in enumerate(jnp.split(x, cut_rows(x.shape[cut], count), axis=cut)):
        if piece.size:
            sequence = [(leading - k) % count for k in range(count)]
            done.append(all_blocks(piece, axes, sequence))
    return in_order(jnp.concatenate(done, axis=cut + 1), dim)


def worked_whole(x, axes, dim, apply):
    return apply(gather_at_once(x, axes, dim), jnp.int32(0))


def as_sent(x):
    return jax.tree.map(lambda a: a.astype(jnp.bfloat16) if a.dtype == jnp.float32 else a, x)


def passed_along(x, axis, by):
    length = lax.axis_size(axis)
    pairs = [(i, i + by) for i in range(length) if 0 <= i + by < length]
    return lax.ppermute(x, axis, pairs)


def neutral_like(x, identity):
    return jax.tree.map(
        lambda a, e: jnp.broadcast_to(jnp.asarray(e, a.dtype), a.shape), x, identity
    )


def entering(x, axes, combine, identity, reverse):
    before = start = neutral_like(x, identity)
    subtotal = x
    for axis in reversed(axes):
        length, here = lax.axis_size(axis), lax.axis_index(axis)
        pieces = jax.tree.map(lambda part: lax.all_gather(part, axis), subtotal)
        inside, subtotal = start, start
        for k in reversed(range(length)) if reverse else range(length):
            passed = k > here if reverse else k < here
            subtotal = combine(subtotal, jax.tree.map(lambda part: part[k], pieces))
            inside = jax.tree.map(lambda new, old: jnp.where(passed, new, old), subtotal, inside)
        before = combine(inside, before)
    return before


def own_rows(term, span, axes):
    subtotal = term(jnp.int32(0), span * lax.axis_size(axes)).astype(jnp.bfloat16)
    for axis in axes:
        subtotal = lax.psum_scatter(subtotal, axis, scatter_dimension=0, tiled=True)
    return subtotal.astype(jnp.float32)


def unit_inverse(lower):
    size = lower.shape[-1]
    inverse = jnp.eye(size, dtype=jnp.float32) - lower
    power = jnp.matmul(lower, lower, precision=highest)
    span = 2
    while span < size:
        inverse = inverse + jnp.matmul(inverse, power, precision=highest)
        power = jnp.matmul(power, power, precision=highest)
        span = span * 2
    return inverse


def make_terms(query, keys, values, beta, rate_col):
    size = query.shape[-2]
    steps = jnp.arange(1, size + 1).astype(jnp.float32)
    cumulative = -rate_col * steps
    lower_mask = jnp.tril(jnp.ones((size, size), bool))
    strict_mask = jnp.tril(jnp.ones((size, size), bool), -1)
    decay = jnp.where(lower_mask, jnp.exp(cumulative[..., :, None] - cumulative[..., None, :]), 0.0)
    weighted = keys * beta[..., None]
    lower = jnp.where(
        strict_mask,
        jnp.einsum("...cd,...sd->...cs", weighted, keys, precision=highest) * decay,
        0.0,
    )
    inverse = unit_inverse(lower)
    update = jnp.einsum("...cs,...sv->...cv", inverse, values * beta[..., None], precision=highest)
    erase = jnp.einsum(
        "...cs,...sd->...cd", inverse, weighted * jnp.exp(cumulative)[..., None], precision=highest
    )
    scores = jnp.einsum("...cd,...sd->...cs", query, keys, precision=highest) * decay
    query_decayed = query * jnp.exp(cumulative)[..., None]
    final = cumulative[..., -1:]
    keys_decayed = keys * jnp.exp(final - cumulative)[..., None]
    return (query_decayed, keys_decayed, update, erase, scores, jnp.exp(final))


def apply_block(state, terms):
    query_decayed, keys_decayed, update, erase, scores, kept = terms
    fresh = update - jnp.einsum("...cd,...dv->...cv", erase, state, precision=highest)
    output = jnp.einsum("...cd,...dv->...cv", query_decayed, state, precision=highest)
    output = output + jnp.einsum("...cs,...sv->...cv", scores, fresh, precision=highest)
    state = state * kept[..., None] + jnp.einsum(
        "...cd,...cv->...dv", keys_decayed, fresh, precision=highest
    )
    return (state, output)


def causal_conv(pre, conv_taps, history):
    width = conv_taps.shape[0]
    extended = jnp.concatenate([history, pre], axis=0).astype(jnp.float32)
    length = pre.shape[0]
    total = jnp.zeros(pre.shape, jnp.float32)
    for tap in range(width):
        total = total + extended[tap : tap + length] * conv_taps[tap].astype(jnp.float32)
    return total


def rms_scale(values_in, gain):
    values = values_in.astype(jnp.float32)
    scaled = values * lax.rsqrt(jnp.mean(values * values, axis=-1, keepdims=True) + epsilon)
    return (scaled * gain).astype(jnp.bfloat16)


def l2_normalize(array):
    return array * lax.rsqrt(jnp.sum(array * array, axis=-1, keepdims=True) + epsilon)


def finish(outputs, out_gain, gate_pre):
    normed = (
        outputs
        * lax.rsqrt(jnp.mean(outputs * outputs, axis=-1, keepdims=True) + out_epsilon)
        * out_gain
    )
    gate = jax.nn.silu(gate_pre.astype(jnp.float32)).reshape(outputs.shape)
    return (normed * gate).astype(jnp.bfloat16).reshape(outputs.shape[0], outputs.shape[1], -1)


def compose(earlier, later):
    first_map, first_shift = earlier
    second_map, second_shift = later
    joined_map = jnp.einsum("shde,shef->shdf", second_map, first_map, precision=highest)
    joined_shift = (
        jnp.einsum("shde,shev->shdv", second_map, first_shift, precision=highest) + second_shift
    )
    return (joined_map, joined_shift)


def shards(
    tokens,
    in_gain,
    w_query,
    w_key,
    w_value,
    w_gate,
    w_beta,
    conv_query,
    conv_key,
    conv_value,
    decay_rate,
    out_gain,
    w_out,
):
    rows = tokens.shape[0]
    seq_count = tokens.shape[1]
    width = tokens.shape[2]
    head_width = w_query.shape[1]
    local_heads = w_beta.shape[1]
    depth = head_width // local_heads
    normed = rms_scale(tokens, in_gain)
    full_query, full_key, full_value, full_gate, full_beta = one_gather(
        (w_query, w_key, w_value, w_gate, w_beta), SP, (0, 0, 0, 0, 0)
    )
    full_out = gather_axes(w_out, SP, 1)

    def project(piece, start):
        flat = piece.reshape(-1, width)
        parts = [
            jnp.dot(flat, weight, preferred_element_type=jnp.float32).astype(jnp.bfloat16)
            for weight in (full_query, full_key, full_value, full_gate, full_beta)
        ]
        return jnp.concatenate(parts, axis=1).reshape(piece.shape[0], seq_count, -1)

    projected = worked_whole(normed, TP, 0, project)
    span = projected.shape[0]
    mixed_pre = projected[:, :, : 3 * head_width]
    gate_pre = projected[:, :, 3 * head_width : 4 * head_width]
    beta_pre = projected[:, :, 4 * head_width :]
    taps = conv_query.shape[0]
    history = passed_along(as_sent(mixed_pre[span - taps + 1 :]), SP, 1)
    conv_taps = jnp.concatenate([conv_query, conv_key, conv_value], axis=1)
    convolved = jax.nn.silu(causal_conv(mixed_pre, conv_taps, history))

    def split_heads(array):
        return array.reshape(span, seq_count, local_heads, depth)

    query = l2_normalize(split_heads(convolved[:, :, :head_width])) * depth ** (-0.5)
    keys = l2_normalize(split_heads(convolved[:, :, head_width : 2 * head_width]))
    values = split_heads(convolved[:, :, 2 * head_width :])
    total_tokens = span * lax.axis_size(SP)
    beta = jax.nn.sigmoid(beta_pre.astype(jnp.float32) + math.log(depth / (4.0 * total_tokens)))
    rate_col = (decay_rate / total_tokens)[:, None]
    blocks = span // BLOCK

    def to_blocks(array):
        return jnp.moveaxis(array.reshape(blocks, BLOCK, seq_count, local_heads, depth), 1, 3)

    beta_blocks = jnp.moveaxis(beta.reshape(blocks, BLOCK, seq_count, local_heads), 1, 3)
    query_decayed, keys_decayed, update, erase, scores, kept = make_terms(
        to_blocks(query), to_blocks(keys), to_blocks(values), beta_blocks, rate_col
    )
    identity = jnp.broadcast_to(
        jnp.eye(depth, dtype=jnp.float32), (seq_count, local_heads, depth, depth)
    )
    zeros = jnp.zeros((seq_count, local_heads, depth, depth), jnp.float32)
    transfer = identity
    offset = zeros
    local_outputs = []
    readouts = []
    for index in range(blocks):
        block_terms = (
            query_decayed[index],
            keys_decayed[index],
            update[index],
            erase[index],
            scores[index],
            kept,
        )
        offset_next, output = apply_block(offset, block_terms)
        local_outputs.append(output)
        reach = query_decayed[index] - jnp.einsum(
            "shct,shtd->shcd", scores[index], erase[index], precision=highest
        )
        readouts.append(jnp.einsum("shcd,shde->shce", reach, transfer, precision=highest))
        erased = jnp.einsum("shcd,shde->shce", erase[index], transfer, precision=highest)
        transfer = transfer * kept[..., None] - jnp.einsum(
            "shcd,shce->shde", keys_decayed[index], erased, precision=highest
        )
        offset = offset_next
    prefix = entering((as_sent(transfer), as_sent(offset)), SP, compose, (identity, zeros), False)
    incoming = prefix[1]
    outputs = jnp.stack(local_outputs) + jnp.einsum(
        "nshcd,shdv->nshcv", jnp.stack(readouts), incoming, precision=highest
    )
    outputs = jnp.moveaxis(outputs, 3, 1).reshape(span, seq_count, local_heads, depth)
    gated = finish(outputs, out_gain, gate_pre)

    def head_term(start, count_rows):
        block = lax.dynamic_slice_in_dim(gated, start, count_rows, 0)
        flat = block.reshape(-1, head_width)
        return jnp.dot(flat, full_out, preferred_element_type=jnp.float32).reshape(
            count_rows, seq_count, -1
        )

    summed = own_rows(head_term, rows, TP)
    return summed.astype(jnp.bfloat16)


def solution(mesh):
    finer = Mesh(mesh.devices.reshape(16, 4, 4, 2), ("sp_0", "sp_1", "tp_0", "tp_1"))
    return jax.shard_map(
        shards,
        mesh=finer,
        in_specs=(
            P(SP_TP, None, None),
            P(),
            P(SP, TP),
            P(SP, TP),
            P(SP, TP),
            P(SP, TP),
            P(SP, TP),
            P(None, TP),
            P(None, TP),
            P(None, TP),
            P(TP),
            P(),
            P(TP, SP),
        ),
        out_specs=P(SP_TP, None, None),
        check_vma=False,
    )
```

profile of v0, /device:TPU:1, one launch (start us, length us, event | category | flops | bytes accessed | tf_op | source)
XLA Modules:
  0.0 561.1 jit_solution(10700707237145528193)
XLA Ops:
  7.3 1.3 dynamic-slice
  12.5 1.0 copy-done.1
  15.7 8.3 %all-gather.2 = bf16[12,4,1024]{2,1,0:T(4,128)(2,1)S(1)} all-gather(bf16[6,4,1024]{2,1,0:T(4,128)(2,1)S(1)} %get-tuple-element.19), channel_id=4, replica_groups=mesh['sp_0'=16,'sp_1'=4,'tp_0'=4,'tp_1'=2] {'tp_1'}, dimensions={0}, use_global_device_ids=true | all-gather | bytes 147456 | tf_op jit(solution)/shard_map/all_gather | solution.py:51
  24.0 9.2 %all-gather = bf16[24,4,1024]{2,1,0:T(4,128)(2,1)S(1)} all-gather(bf16[6,4,1024]{2,1,0:T(4,128)(2,1)S(1)} %get-tuple-element.18), channel_id=2, replica_groups=mesh['sp_0'=16,'sp_1'=4,'tp_0'=4,'tp_1'=2] {'tp_0'}, dimensions={0}, use_global_device_ids=true | all-gather | bytes 245760 | tf_op jit(solution)/shard_map/all_gather | solution.py:51
  33.3 5.0 all-gather.1
  38.4 10.2 %all-gather.3 = bf16[8,6,4,1024]{3,2,1,0:T(4,128)(2,1)S(1)} all-gather(bf16[2,6,4,1024]{3,2,1,0:T(4,128)(2,1)S(1)} %bitcast.294), channel_id=5, replica_groups=mesh['sp_0'=16,'sp_1'=4,'tp_0'=4,'tp_1'=2] {'tp_0'}, dimensions={0}, use_global_device_ids=true | all-gather | bytes 491520 | tf_op jit(solution)/shard_map/all_gather | solution.py:51
  50.3 237.1 %all-reduce.5.cloned.1.call-done = bf16[525312]{0:T(1024)(128)(2,1)} async-done(((bf16[525312]{0:T(1024)(128)(2,1)}), bf16[525312]{0:T(1024)(128)(2,1)}) %all-reduce.5.cloned.1.call-update) | async-done | bytes 1050640
  287.3 2.6 reshape.857
  292.2 1.8 collective-permute-start
  298.4 10.4 %all-gather.5 = bf16[16,128,128]{2,1,0:T(8,128)(2,1)S(1)} all-gather(bf16[4,128,128]{2,1,0:T(8,128)(2,1)S(1)} %fusion.1), channel_id=7, replica_groups=mesh['sp_0'=16,'sp_1'=4,'tp_0'=4,'tp_1'=2] {'sp_1'}, dimensions={0}, use_global_device_ids=true | all-gather | bytes 655360 | tf_op jit(solution)/shard_map/all_gather | solution.py:93
  312.3 11.3 %all-gather.7 = bf16[16,128,128]{2,1,0:T(8,128)(2,1)S(1)} all-gather(bf16[4,128,128]{2,1,0:T(8,128)(2,1)S(1)} %fusion.2), channel_id=9, replica_groups=mesh['sp_0'=16,'sp_1'=4,'tp_0'=4,'tp_1'=2] {'sp_1'}, dimensions={0}, use_global_device_ids=true | all-gather | bytes 655360 | tf_op jit(solution)/shard_map/all_gather | solution.py:93
  325.3 1.1 convolution_add_fusion.23
  327.9 9.3 %all_gather.78 = bf16[128,64]{0,1:T(8,128)(2,1)S(1)} all-gather(bf16[128,16]{0,1:T(8,128)(2,1)S(1)} %copy-done.18), channel_id=1, replica_groups=mesh['sp_0'=16,'sp_1'=4,'tp_0'=4,'tp_1'=2] {'sp_1'}, dimensions={1}, use_global_device_ids=true | all-gather | bytes 20480 | tf_op jit(solution)/shard_map/all_gather | solution.py:39
  337.2 27.0 %all_gather.79 = bf16[128,1024]{0,1:T(8,128)(2,1)S(1)} all-gather(bf16[128,64]{0,1:T(8,128)(2,1)S(1)} %all_gather.78), channel_id=1, replica_groups=mesh['sp_0'=16,'sp_1'=4,'tp_0'=4,'tp_1'=2] {'sp_0'}, dimensions={1}, use_global_device_ids=true | all-gather | bytes 278528 | tf_op jit(solution)/shard_map/all_gather | solution.py:39
  367.3 0.9 convolution_bitcast_fusion.2
  369.0 18.6 %all-gather.12.cloned.1.call-done = bf16[64,128,128]{2,1,0:T(8,128)(2,1)} async-done(((bf16[4,128,128]{2,1,0:T(8,128)(2,1)}), bf16[64,128,128]{2,1,0:T(8,128)(2,1)}) %all-gather.12.cloned.1.call-update) | async-done | bytes 2097168 | tf_op jit(solution)/shard_map/all_gather | solution.py:93
  387.6 71.7 %all-gather.14.cloned.1.call-done = bf16[64,128,128]{2,1,0:T(8,128)(2,1)} async-done(((bf16[4,128,128]{2,1,0:T(8,128)(2,1)}), bf16[64,128,128]{2,1,0:T(8,128)(2,1)}) %all-gather.14.cloned.1.call-update) | async-done | bytes 2097168 | tf_op jit(solution)/shard_map/all_gather | solution.py:93
  459.3 1.3 convolution_add_fusion.26
  460.6 1.1 convolution_add_fusion.21
  461.7 1.1 convolution_add_fusion.20
  462.9 1.1 convolution_add_fusion.19
  464.0 1.1 convolution_add_fusion.18
  465.1 1.1 convolution_add_fusion.17
  467.8 1.0 fusion.9
  468.8 1.2 fusion.11
  470.1 1.3 multiply_reduce_fusion
  471.9 1.0 copy.53
  473.0 34.6 %reduce-scatter.4.cloned.1.call-done = bf16[24,4096]{1,0:T(8,128)(2,1)} async-done(((bf16[96,4096]{1,0:T(8,128)(2,1)}), bf16[24,4096]{1,0:T(8,128)(2,1)}) %reduce-scatter.4.cloned.1.call-update) | async-done | bytes 196624
  507.6 1.7 reshape.954
  509.4 1.3 dynamic-slice.1
  511.3 41.7 %all-reduce.7.cloned.1.call-done = bf16[24,4,1024]{2,1,0:T(4,128)(2,1)} async-done(((bf16[24,4,1024]{2,1,0:T(4,128)(2,1)}), bf16[24,4,1024]{2,1,0:T(4,128)(2,1)}) %all-reduce.7.cloned.1.call-update) | async-done | bytes 196624
  553.0 1.6 constant_dynamic-slice_fusion
  (164 shorter events, 25.6 us)
Async XLA Ops:
  6.5 8.8 %copy-start.21 = (bf16[4,128]{1,0:T(4,128)(2,1)S(1)}, bf16[4,128]{1,0:T(4,128)(2,1)}, u32[]{:S(2)}) copy-start(bf16[4,128]{1,0:T(4,128)(2,1)} %param.20) | copy-start | bytes 3076
  6.5 8.8 %copy-start.9 = (bf16[12,4,1024]{2,1,0:T(4,128)(2,1)S(1)}, bf16[12,4,1024]{2,1,0:T(4,128)(2,1)}, u32[]{:S(2)}) copy-start(bf16[12,4,1024]{2,1,0:T(4,128)(2,1)} %param.13) | copy-start | bytes 294916
  6.5 9.0 %copy-start.17 = (f32[1024]{0:T(1024)S(1)}, f32[1024]{0:T(1024)}, u32[]{:S(2)}) copy-start(f32[1024]{0:T(1024)} %param.14) | copy-start | bytes 12292
  6.5 280.8 %all-reduce.5.cloned.1.call-start = ((), (), s32[]{:S(2)}) async-start(), calls=%async_computation.3 | async-start | bytes 2101248
  12.0 36.7 %copy-start.22 = (bf16[4,128]{1,0:T(4,128)(2,1)S(1)}, bf16[4,128]{1,0:T(4,128)(2,1)}, u32[]{:S(2)}) copy-start(bf16[4,128]{1,0:T(4,128)(2,1)} %param.21) | copy-start | bytes 3076
  12.0 36.7 %copy-start.23 = (bf16[4,128]{1,0:T(4,128)(2,1)S(1)}, bf16[4,128]{1,0:T(4,128)(2,1)}, u32[]{:S(2)}) copy-start(bf16[4,128]{1,0:T(4,128)(2,1)} %param.22) | copy-start | bytes 3076
  12.5 1.0 copy-start.1
  13.5 374.1 %all-gather.12.cloned.1.call-start = ((), (), s32[]{:S(2)}) async-start(), calls=%async_computation.1 | async-start | bytes 2228224 | tf_op jit(solution)/shard_map/all_gather | solution.py:93
  14.2 283.1 %copy-start.19 = (f32[32]{0:T(128)}, f32[32]{0:T(128)S(1)}, u32[]{:S(2)}) copy-start(f32[32]{0:T(128)S(1)} %fusion.124) | copy-start | bytes 388
  50.0 258.8 %copy-start.14 = (bf16[128,128]{1,0:T(8,128)(2,1)}, bf16[128,128]{1,0:T(8,128)(2,1)S(1)}, u32[]{:S(2)}) copy-start(bf16[128,128]{1,0:T(8,128)(2,1)S(1)} %fusion.110) | copy-start | bytes 98308
  50.0 247.5 %copy-start.10 = (bf16[128,128]{1,0:T(8,128)(2,1)}, bf16[128,128]{1,0:T(8,128)(2,1)S(1)}, u32[]{:S(2)}) copy-start(bf16[128,128]{1,0:T(8,128)(2,1)S(1)} %fusion.107) | copy-start | bytes 98308
  292.2 2.6 collective-permute-start
  309.0 1.9 copy-start.4
  310.2 149.0 %all-gather.14.cloned.1.call-start = ((), (), s32[]{:S(2)}) async-start(), calls=%async_computation.2 | async-start | bytes 2228224 | tf_op jit(solution)/shard_map/all_gather | solution.py:93
  311.1 0.6 copy-start.12
  312.3 15.6 %copy-start.18 = (bf16[128,16]{0,1:T(8,128)(2,1)S(1)}, bf16[128,16]{0,1:T(8,128)(2,1)}, u32[]{:S(2)}) copy-start(bf16[128,16]{0,1:T(8,128)(2,1)} %param.25) | copy-start | bytes 12292
  323.8 0.6 copy-start.6
  324.4 40.3 %copy-start.20 = (f32[32]{0:T(128)S(1)}, f32[32]{0:T(128)}, u32[]{:S(2)}) copy-start(f32[32]{0:T(128)} %copy-done.19) | copy-start | bytes 388
  326.3 0.7 copy-start.8
  327.8 38.4 %copy-start.13 = (bf16[4,32,128]{2,1,0:T(8,128)(2,1)S(1)}, bf16[4,32,128]{2,1,0:T(8,128)(2,1)}, u32[]{:S(2)}) copy-start(bf16[4,32,128]{2,1,0:T(8,128)(2,1)} %copy-done.12) | copy-start | bytes 98308
  327.8 179.8 %reduce-scatter.4.cloned.1.call-start = ((), (), s32[]{:S(2)}) async-start(), calls=%async_computation.4 | async-start | bytes 983040
  337.2 29.8 %copy-start.11 = (bf16[128,128]{1,0:T(8,128)(2,1)S(1)}, bf16[128,128]{1,0:T(8,128)(2,1)}, u32[]{:S(2)}) copy-start(bf16[128,128]{1,0:T(8,128)(2,1)} %copy-done.10) | copy-start | bytes 98308
  387.6 75.3 %copy-start = (bf16[64,128,128]{2,1,0:T(8,128)(2,1)S(1)}, bf16[64,128,128]{2,1,0:T(8,128)(2,1)}, u32[]{:S(2)}) copy-start(bf16[64,128,128]{2,1,0:T(8,128)(2,1)} %all-gather.12.cloned.1.call-done) | copy-start | bytes 6291460
  459.3 6.8 %copy-start.2 = (bf16[64,128,128]{2,1,0:T(8,128)(2,1)S(1)}, bf16[64,128,128]{2,1,0:T(8,128)(2,1)}, u32[]{:S(2)}) copy-start(bf16[64,128,128]{2,1,0:T(8,128)(2,1)} %all-gather.14.cloned.1.call-done) | copy-start | bytes 6291460
  467.6 1.2 copy-start.3
  467.6 1.2 copy-start.5
  467.6 1.2 copy-start.15
  467.8 2.2 copy-start.7
  467.8 2.2 copy-start.16
  468.8 2.7 copy-start.24
  472.9 80.0 %all-reduce.7.cloned.1.call-start = ((), (), s32[]{:S(2)}) async-start(), calls=%async_computation.5 | async-start | bytes 393216
Sparse Core Ops, SparseCore 0:
  13.6 273.7 all-reduce.4
  310.4 77.1 all-gather.11
  389.7 69.5 all-gather.13
  473.0 34.5 reduce-scatter.3
  510.3 42.5 all-reduce.6
where the time goes:
time: 562 us; the launch traced here: 561 us
  waiting for transfers between devices  404 us (72%)
  blocking collectives  90.7 us (16%)
  matrix products  26.4 us (5%)
  local copies, waits for them, and re-layouts  18.4 us (3%)
  between operations  16.6 us (3%)
    unnamed x8, waiting for transfers between devices  313 us
    all_gather x2, waiting for transfers between devices, entering(): pieces = jax.tree.map(lambda part: lax.all_gather(part, axis), subtotal)  90.3 us
    all_gather x2, blocking collectives, gather_axes(): filled = lax.all_gather(filled, axes[number], axis=dim, tiled=True)  36.2 us
    all_gather x4, blocking collectives, all_blocks(): pieces = lax.all_gather(pieces, axes[k])  32.8 us
    all_gather x2, blocking collectives, entering(): pieces = jax.tree.map(lambda part: lax.all_gather(part, axis), subtotal)  21.7 us
    dot_general x21, matrix products, compose(): jnp.einsum('shde,shev->shdv', second_map, first_shift, precision=highest)  13.4 us
    unnamed x64, local copies, waits for them, and re-layouts  11.4 us
  transfers between devices with their start and end apart: 6, of which 6 were waited for; matrix products, arithmetic and copies ran while one was open for 2% of the time, Pallas kernels for 0%

commit v1 on v0

v1 whole, which is shorter than its diff:
```python
import functools
import math

import jax
import jax.numpy as jnp
from jax import lax
from jax.experimental import pallas as pl
from jax.experimental.pallas import tpu as pltpu
from jax.sharding import Mesh
from jax.sharding import PartitionSpec as P

MESH = pl.DeviceIdType.MESH
DK = 128
TAPS = 4
INNER = 32
ROWS = 16
f32, bf16 = jnp.float32, jnp.bfloat16
epsilon = 1e-06
out_epsilon = 1e-10
SP = ("z", "y")
TP = ("x", "c")


def copy_to(src, dst, send, recv, device):
    return pltpu.make_async_remote_copy(
        src_ref=src, dst_ref=dst, send_sem=send, recv_sem=recv, device_id=device, device_id_type=MESH
    )


def dot(a, b):
    return jnp.dot(a.astype(bf16), b.astype(bf16), preferred_element_type=f32)


def dot_nt(a, b):
    return lax.dot_general(
        a.astype(bf16), b.astype(bf16), (((1,), (1,)), ((), ())), preferred_element_type=f32
    )


def mixer(
    dims, x_ref, w_ref, b_ref, taps_ref, rate_ref, gain_ref, out_ref,
    wbuf, bbuf, wbt, xbuf, hin, ext, bext, qs, ks, vs, bs, olo, rdo, mbuf, wo, gsend, grecv, obuf,
    wy_s, wy_r, by_s, by_r, wz_s, wz_r, bz_s, bz_r, xy_s, xy_r, hz_s, hz_r, hy_s, hy_r, hx_s, hx_r,
    hc_s, hc_r, xx_s, xx_r, xc_s, xc_r, ox_s, ox_r, oc_s, oc_r, mz_s, mz_r, g_s, g_r, o_s, o_r, l_s,
):
    Z, Y, X, NB, PB, CH = dims
    TPN = 2 * X
    NT = Y * TPN * NB
    D = wo.shape[2]
    z, y, x, c = (lax.axis_index(a) for a in ("z", "y", "x", "c"))
    tp = x * 2 + c
    NP, NM = Z // 2, (Z - 1) // 2
    up = (lax.rem(z + 1, Z), y, x, c)
    down = (lax.rem(z + Z - 1, Z), y, x, c)
    sib = (z, y, x, 1 - c)

    def ymod(k):
        return lax.rem(y + k, Y)

    def xmod(k):
        return lax.rem(x + k, X)

    def zmod(k):
        return lax.rem(z + k + Z, Z)

    barrier = pltpu.get_barrier_semaphore()
    peers = [up, down] + [(z, ymod(k), x, c) for k in range(1, Y)]
    peers += [(z, y, lax.rem(tp + k, TPN) // 2, lax.rem(lax.rem(tp + k, TPN), 2)) for k in range(1, TPN)]
    for peer in peers:
        pl.semaphore_signal(barrier, inc=1, device_id=peer, device_id_type=MESH)
    pl.semaphore_wait(barrier, len(peers))

    copies = []

    def go(cp):
        cp.start()
        copies.append(cp)

    def rows_of(zz, yy):
        return pl.ds(pl.multiple_of((zz * Y + yy) * ROWS, ROWS), ROWS)

    own = rows_of(z, y)
    local = pltpu.make_async_copy(w_ref, wbuf.at[own], l_s.at[0])
    local.start()
    local_b = pltpu.make_async_copy(b_ref, bbuf.at[z, y], l_s.at[1])
    local_b.start()
    for k in range(1, Y):
        go(copy_to(w_ref, wbuf.at[own], wy_s.at[k], wy_r.at[k], (z, ymod(k), x, c)))
        go(copy_to(b_ref, bbuf.at[z, y], by_s.at[k], by_r.at[k], (z, ymod(k), x, c)))
    go(copy_to(w_ref, wbuf.at[own], wz_s.at[0, 1, 0], wz_r.at[0, 1, 0], up))
    if NM:
        go(copy_to(w_ref, wbuf.at[own], wz_s.at[1, 1, 0], wz_r.at[1, 1, 0], down))
    slot0 = tp * Y
    for k in range(1, Y):
        go(copy_to(x_ref.at[ymod(k)], xbuf.at[slot0 + y], xy_s.at[k], xy_r.at[k], (z, ymod(k), x, c)))
    local_x = pltpu.make_async_copy(x_ref.at[y], xbuf.at[slot0 + y], l_s.at[2])
    local_x.start()
    HALO = TPN * Y
    last_tp = jnp.logical_and(x == X - 1, c == 1)
    tail_owner = jnp.logical_and(last_tp, y == Y - 1)

    @pl.when(tail_owner)
    def _():
        copy_to(x_ref, hin, hz_s, hz_r, up).start()

    for k in range(1, Y):
        blk = rows_of(z, ymod(Y - k))
        copy_to(w_ref, wbuf.at[blk], wy_s.at[k], wy_r.at[k], sib).wait_recv()
    for d in range(1, Y):
        blk = rows_of(z, ymod(d))
        go(copy_to(wbuf.at[blk], wbuf.at[blk], wz_s.at[0, 1, d], wz_r.at[0, 1, d], up))
        if NM:
            go(copy_to(wbuf.at[blk], wbuf.at[blk], wz_s.at[1, 1, d], wz_r.at[1, 1, d], down))
    for k in range(1, Y):
        copy_to(b_ref, bbuf.at[z, ymod(Y - k)], by_s.at[k], by_r.at[k], sib).wait_recv()
    local_b.wait()
    go(copy_to(bbuf.at[z], bbuf.at[z], bz_s.at[0, 1], bz_r.at[0, 1], up))
    if NM:
        go(copy_to(bbuf.at[z], bbuf.at[z], bz_s.at[1, 1], bz_r.at[1, 1], down))

    for k in range(1, Y):
        copy_to(x_ref.at[0], xbuf.at[slot0 + ymod(Y - k)], xy_s.at[k], xy_r.at[k], sib).wait_recv()
    local_x.wait()
    mine = pl.ds(slot0, Y)
    for k in range(1, X):
        go(copy_to(xbuf.at[mine], xbuf.at[mine], xx_s.at[k], xx_r.at[k], (z, y, xmod(k), c)))
    go(copy_to(xbuf.at[mine], xbuf.at[mine], xc_s.at[0], xc_r.at[0], sib))

    def w_step(k, plus, fplus, minus, fminus):
        for d in range(Y):
            if plus:
                blk = rows_of(zmod(-k), ymod(d))
                copy_to(wbuf.at[blk], wbuf.at[blk], wz_s.at[0, k, d], wz_r.at[0, k, d], up).wait_recv()
                if fplus:
                    copy_to(wbuf.at[blk], wbuf.at[blk], wz_s.at[0, k + 1, d], wz_r.at[0, k + 1, d], up).start()
            if minus:
                blk = rows_of(zmod(k), ymod(d))
                copy_to(wbuf.at[blk], wbuf.at[blk], wz_s.at[1, k, d], wz_r.at[1, k, d], down).wait_recv()
                if fminus:
                    copy_to(wbuf.at[blk], wbuf.at[blk], wz_s.at[1, k + 1, d], wz_r.at[1, k + 1, d], down).start()
        if plus:
            g = bbuf.at[zmod(-k)]
            copy_to(g, g, bz_s.at[0, k], bz_r.at[0, k], up).wait_recv()
            if fplus:
                copy_to(g, g, bz_s.at[0, k + 1], bz_r.at[0, k + 1], up).start()
        if minus:
            g = bbuf.at[zmod(k)]
            copy_to(g, g, bz_s.at[1, k], bz_r.at[1, k], down).wait_recv()
            if fminus:
                copy_to(g, g, bz_s.at[1, k + 1], bz_r.at[1, k + 1], down).start()

    def ring(step):
        both = max(min(NP - 1, NM - 1), 0)
        if both:

            @pl.loop(1, both + 1)
            def _(k):
                step(k, True, True, True, True)

        for k in range(both + 1, NP + 1):
            step(k, True, k < NP, k <= NM, k < NM)

    def token_forwards():
        @pl.when(tail_owner)
        def _():
            copy_to(x_ref, hin, hz_s, hz_r, up).wait_recv()
            for k in range(1, Y):
                copy_to(hin.at[ymod(k)], xbuf.at[HALO], hy_s.at[k], hy_r, (z, ymod(k), x, c)).start()
            cp = pltpu.make_async_copy(hin.at[y], xbuf.at[HALO], l_s.at[3])
            cp.start()
            cp.wait()

        @pl.when(jnp.logical_and(last_tp, y != Y - 1))
        def _():
            copy_to(hin.at[0], xbuf.at[HALO], hy_s.at[0], hy_r, sib).wait_recv()

        @pl.when(last_tp)
        def _():
            for k in range(1, X):
                copy_to(xbuf.at[HALO], xbuf.at[HALO], hx_s.at[k], hx_r, (z, y, xmod(k), c)).start()

        for k in range(1, X):
            got = pl.ds((xmod(X - k) * 2 + c) * Y, Y)
            copy_to(xbuf.at[got], xbuf.at[got], xx_s.at[k], xx_r.at[k], sib).wait_recv()
            go(copy_to(xbuf.at[got], xbuf.at[got], xc_s.at[k], xc_r.at[k], sib))

        @pl.when(c == 1)
        def _():
            @pl.when(x != X - 1)
            def _():
                copy_to(xbuf.at[HALO], xbuf.at[HALO], hx_s.at[0], hx_r, sib).wait_recv()

            copy_to(xbuf.at[HALO], xbuf.at[HALO], hc_s, hc_r, sib).start()

    w_step_early = min(2, NP - 1)
    token_forwards()
    ring(w_step)

    sc = (1 - c)
    for k in range(X):
        got = pl.ds((xmod(X - k) * 2 + sc) * Y, Y)
        copy_to(xbuf.at[got], xbuf.at[got], xc_s.at[k], xc_r.at[k], sib).wait_recv()

    @pl.when(c == 0)
    def _():
        copy_to(xbuf.at[HALO], xbuf.at[HALO], hc_s, hc_r, sib).wait_recv()

    local.wait()

    PR = TPN * Y * PB
    xs = xbuf[...].reshape(PR + PB, D)
    pre = jnp.dot(xs, wbuf[:, : 4 * DK], preferred_element_type=f32).astype(bf16).astype(f32)
    bsum = jnp.sum(bbuf[...].reshape(D // DK, 8, DK), axis=1)
    for j in range(D // DK):
        wbt[:, j * DK : (j + 1) * DK] = jnp.broadcast_to(bsum[j : j + 1, :], (DK, DK)).astype(bf16)
    bpre = dot_nt(xs, wbt[...]).astype(bf16).astype(f32)
    started = jnp.where(z > 0, 1.0, 0.0).astype(f32)
    ext[8 - (TAPS - 1) : 8, :] = pre[PR + NB - (TAPS - 1) : PR + NB, :] * started
    for yy in range(Y):
        for t in range(TPN):
            row = (t * Y + yy) * PB
            to = (yy * TPN + t) * NB
            ext[8 + to : 8 + to + NB, :] = pre[row : row + NB, :]
            bext[to : to + NB, :] = bpre[row : row + NB, :]

    for j in range(D // DK):
        tile = wbuf[j * DK : (j + 1) * DK, 4 * DK : 5 * DK].astype(f32)
        wo[tp, :, j * DK : (j + 1) * DK] = tile.T.astype(bf16)

    outs = []
    for kind in range(3):
        lanes = slice(kind * DK, (kind + 1) * DK)
        acc = jnp.zeros((NT, DK), f32)
        for j in range(TAPS):
            at = 8 - (TAPS - 1) + j
            acc = acc + ext[at : at + NT, lanes] * taps_ref[j : j + 1, lanes]
        outs.append(acc * jax.nn.sigmoid(acc))
    q, k_, v = outs
    qs[...] = q * (lax.rsqrt(jnp.sum(q * q, axis=1, keepdims=True) + epsilon) * DK ** (-0.5))
    ks[...] = k_ * lax.rsqrt(jnp.sum(k_ * k_, axis=1, keepdims=True) + epsilon)
    vs[...] = v
    total_tokens = NT * Z
    bs[...] = jax.nn.sigmoid(bext[...] + math.log(DK / (4.0 * total_tokens)))

    for k in range(1, X):
        go(copy_to(wo.at[tp], wo.at[tp], ox_s.at[k], ox_r.at[k], (z, y, xmod(k), c)))
    go(copy_to(wo.at[tp], wo.at[tp], oc_s.at[0], oc_r.at[0], sib))

    rate = rate_ref[...]
    ri = lax.broadcasted_iota(jnp.int32, (CH, CH), 0)
    ci = lax.broadcasted_iota(jnp.int32, (CH, CH), 1)
    rl = lax.broadcasted_iota(jnp.int32, (CH, DK), 0).astype(f32)
    rate_c = rate_ref[:, :CH]
    decay = jnp.where(ri >= ci, jnp.exp(-rate_c * (ri - ci).astype(f32)), 0.0)
    down_row = jnp.exp(-rate * (rl + 1.0))
    up_row = jnp.exp(-rate * (CH - 1.0 - rl))
    kept = jnp.exp(-rate * CH)
    eye = jnp.where(
        lax.broadcasted_iota(jnp.int32, (DK, DK), 0) == lax.broadcasted_iota(jnp.int32, (DK, DK), 1), 1.0, 0.0
    ).astype(f32)
    prefix = None
    for i in range(NT // CH):
        rows = slice(i * CH, (i + 1) * CH)
        q, k_, v, b = qs[rows, :], ks[rows, :], vs[rows, :], bs[rows, :]
        kb = k_ * b
        lower = jnp.where(ri > ci, dot_nt(kb, k_) * decay, 0.0)
        scores = dot_nt(q, k_) * decay
        near = jnp.where(ri // INNER == ci // INNER, lower, 0.0)
        inverse = jnp.where(ri == ci, 1.0, 0.0) - near
        power = dot(near, near)
        span = 2
        while span < INNER:
            inverse = inverse + dot(inverse, power)
            span *= 2
            if span < INNER:
                power = dot(power, power)
        span = INNER
        while span < CH:
            part = jnp.where(
                jnp.logical_and(ri // (2 * span) == ci // (2 * span), ri // span != ci // span), lower, 0.0
            )
            inverse = inverse - dot(inverse, dot(part, inverse))
            span *= 2
        both = dot(inverse, jnp.concatenate([kb * down_row, v * b], axis=1))
        inner = dot(scores, both)
        reach = q * down_row - inner[:, :DK]
        kd = (k_ * up_row).T
        tail = dot(kd, both)
        step_map = kept * eye - tail[:, :DK]
        if prefix is None:
            rdo[rows, :] = reach
            olo[rows, :] = inner[:, DK:]
            prefix = jnp.concatenate([step_map, tail[:, DK:]], axis=1)
        else:
            seen = dot(reach, prefix)
            rdo[rows, :] = seen[:, :DK]
            olo[rows, :] = inner[:, DK:] + seen[:, DK:]
            prefix = dot(step_map, prefix)
            prefix = jnp.concatenate([prefix[:, :DK], prefix[:, DK:] + tail[:, DK:]], axis=1)
    kappa = jnp.exp(-rate * NT)
    mbuf[z, :, :DK] = (prefix[:, :DK] - kappa * eye).astype(bf16)
    mbuf[z, :, DK:] = prefix[:, DK:].astype(bf16)

    NCH = mz_s.shape[2]
    PIECE = DK // NCH

    def piece(zz, d):
        return mbuf.at[zz, pl.ds(d * PIECE, PIECE)]

    for d in range(NCH):
        go(copy_to(piece(z, d), piece(z, d), mz_s.at[0, 1, d], mz_r.at[0, 1, d], up))
        if NM:
            go(copy_to(piece(z, d), piece(z, d), mz_s.at[1, 1, d], mz_r.at[1, 1, d], down))

    near_d, near_u, far = ext.at[0:DK, 0:DK], ext.at[0:DK, DK : 2 * DK], ext.at[0:DK, 2 * DK : 3 * DK]

    near_d[...] = jnp.zeros((DK, DK), f32)
    near_u[...] = jnp.zeros((DK, DK), f32)
    far[...] = jnp.zeros((DK, DK), f32)

    def m_step(k, plus, fplus, minus, fminus):
        for d in range(NCH):
            if plus:
                p = piece(zmod(-k), d)
                copy_to(p, p, mz_s.at[0, k, d], mz_r.at[0, k, d], up).wait_recv()
                if fplus:
                    copy_to(p, p, mz_s.at[0, k + 1, d], mz_r.at[0, k + 1, d], up).start()
            if minus:
                p = piece(zmod(k), d)
                copy_to(p, p, mz_s.at[1, k, d], mz_r.at[1, k, d], down).wait_recv()
                if fminus:
                    copy_to(p, p, mz_s.at[1, k + 1, d], mz_r.at[1, k + 1, d], down).start()
        if plus:
            got = mbuf[zmod(-k)]
            kk = k * 1.0 if isinstance(k, int) else k.astype(f32)
            scale = jnp.exp(-rate * NT * (kk - 1.0))
            valid = jnp.where(z >= k, 1.0, 0.0).astype(f32)
            nd, nu = near_d[...], near_u[...]
            prod = dot(nd, got)
            gd, gu = got[:, :DK].astype(f32), got[:, DK:].astype(f32)
            near_d[...] = kappa * nd + scale * gd + prod[:, :DK]
            near_u[...] = nu + valid * (scale * gu + prod[:, DK:])
        if minus:
            got = mbuf[zmod(k)]
            valid = jnp.where(z + k >= Z, 1.0, 0.0).astype(f32)
            s = far[...]
            far[...] = kappa * s + dot(got[:, :DK], s) + valid * got[:, DK:].astype(f32)

    ring(m_step)

    for k in range(1, X):
        h = xmod(X - k) * 2 + c
        copy_to(wo.at[h], wo.at[h], ox_s.at[k], ox_r.at[k], sib).wait_recv()
        go(copy_to(wo.at[h], wo.at[h], oc_s.at[k], oc_r.at[k], sib))

    s = far[...]
    state = jnp.exp(-rate * NT * NP) * s + dot(near_d[...], s) + near_u[...]
    o = olo[...] + dot(rdo[...], state)
    gate = ext[8 : 8 + NT, 3 * DK : 4 * DK]
    o = o * lax.rsqrt(jnp.mean(o * o, axis=1, keepdims=True) + out_epsilon) * gain_ref[...]
    olo[...] = o * (gate * jax.nn.sigmoid(gate))
    for yy in range(Y):
        for t in range(TPN):
            to = (yy * TPN + t) * NB
            gsend[t, yy, 0:NB, :] = olo[to : to + NB, :].astype(bf16)
    for k in range(1, TPN):
        t = lax.rem(tp + k, TPN)
        go(copy_to(gsend.at[t], grecv.at[tp], g_s.at[k], g_r.at[k], (z, y, t // 2, lax.rem(t, 2))))
    grecv[tp] = gsend[tp]
    for k in range(X):
        h = xmod(X - k) * 2 + sc
        copy_to(wo.at[h], wo.at[h], oc_s.at[k], oc_r.at[k], sib).wait_recv()
    for k in range(1, TPN):
        t = lax.rem(tp + TPN - k, TPN)
        copy_to(gsend.at[0], grecv.at[t], g_s.at[k], g_r.at[k], sib).wait_recv()
    gated = jnp.concatenate([grecv[t].reshape(Y * PB, DK) for t in range(TPN)], axis=1)
    res = jnp.dot(gated, wo[...].reshape(TPN * DK, D), preferred_element_type=f32)
    obuf[0] = res.astype(bf16).reshape(Y, PB, D)
    for k in range(1, Y):
        go(copy_to(obuf.at[0, ymod(k)], obuf.at[1, y], o_s.at[k], o_r.at[k], (z, ymod(k), x, c)))
    out_ref[y] = obuf[0, y]
    for k in range(1, Y):
        src = ymod(Y - k)
        copy_to(obuf.at[0, 0], obuf.at[1, src], o_s.at[k], o_r.at[k], sib).wait_recv()
        out_ref[src] = obuf[1, src]

    for cp in copies:
        cp.wait_send()
    for d, steps in ((0, NP), (1, NM)):
        for k in range(2, steps + 1):
            to = up if d == 0 else down
            for e in range(Y):
                copy_to(w_ref, wbuf.at[own], wz_s.at[d, k, e], wz_r.at[d, k, e], to).wait_send()
            copy_to(bbuf.at[0], bbuf.at[0], bz_s.at[d, k], bz_r.at[d, k], to).wait_send()
            for e in range(NCH):
                copy_to(piece(z, e), piece(z, e), mz_s.at[d, k, e], mz_r.at[d, k, e], to).wait_send()

    @pl.when(tail_owner)
    def _():
        copy_to(x_ref, hin, hz_s, hz_r, up).wait_send()
        for k in range(1, Y):
            copy_to(hin.at[0], xbuf.at[HALO], hy_s.at[k], hy_r, sib).wait_send()

    @pl.when(last_tp)
    def _():
        for k in range(1, X):
            copy_to(xbuf.at[HALO], xbuf.at[HALO], hx_s.at[k], hx_r, sib).wait_send()

    @pl.when(c == 1)
    def _():
        copy_to(xbuf.at[HALO], xbuf.at[HALO], hc_s, hc_r, sib).wait_send()


def shards(
    sizes, tokens, in_gain, w_query, w_key, w_value, w_gate, w_beta,
    conv_query, conv_key, conv_value, decay_rate, out_gain, w_out,
):
    Z, Y, X = sizes
    NB, seqs, D = tokens.shape
    PB = -(-NB // 16) * 16
    TPN = 2 * X
    NT = Y * TPN * NB
    CH = 128 if NT % 128 == 0 else 96
    NCH = 4
    values = tokens.astype(f32)
    scaled = values * lax.rsqrt(jnp.mean(values * values, axis=-1, keepdims=True) + epsilon)
    normed = jnp.swapaxes((scaled * in_gain).astype(bf16), 0, 1)
    normed = jnp.pad(normed, ((0, 0), (0, PB - NB), (0, 0)))
    w = jnp.concatenate([w_query, w_key, w_value, w_gate, w_out.T], axis=1)
    part = lax.rem(lax.axis_index(SP), 8)
    lane = lax.broadcasted_iota(jnp.int32, (1, DK), 1)
    b = jnp.where(lane // ROWS == part, jnp.tile(w_beta.astype(f32).reshape(1, ROWS), (1, 8)), 0.0)
    taps = jnp.concatenate([conv_query, conv_key, conv_value], axis=1).astype(f32)
    rate = jnp.broadcast_to((decay_rate / (NT * Z)).reshape(1, 1), (1, DK))
    D1 = pltpu.SemaphoreType.DMA
    NP = Z // 2
    scratch = [
        pltpu.VMEM((D, 5 * DK), bf16),
        pltpu.VMEM((Z, Y, 1, DK), f32),
        pltpu.VMEM((DK, D), bf16),
        pltpu.VMEM((TPN * Y + 1, PB, D), bf16),
        pltpu.VMEM((Y, PB, D), bf16),
        pltpu.VMEM((8 + max(NT, DK), 4 * DK), f32),
        pltpu.VMEM((NT, DK), f32),
        pltpu.VMEM((NT, DK), f32),
        pltpu.VMEM((NT, DK), f32),
        pltpu.VMEM((NT, DK), f32),
        pltpu.VMEM((NT, DK), f32),
        pltpu.VMEM((NT, DK), f32),
        pltpu.VMEM((NT, DK), f32),
        pltpu.VMEM((Z, DK, 2 * DK), bf16),
        pltpu.VMEM((TPN, DK, D), bf16),
        pltpu.VMEM((TPN, Y, PB, DK), bf16),
        pltpu.VMEM((TPN, Y, PB, DK), bf16),
        pltpu.VMEM((2, Y, PB, D), bf16),
    ]
    sems = [
        D1((Y,)), D1((Y,)), D1((Y,)), D1((Y,)),
        D1((2, NP + 1, Y)), D1((2, NP + 1, Y)), D1((2, NP + 1)), D1((2, NP + 1)),
        D1((Y,)), D1((Y,)), D1(()), D1(()), D1((Y,)), D1(()), D1((X,)), D1(()),
        D1(()), D1(()), D1((X,)), D1((X,)), D1((X,)), D1((X,)),
        D1((X,)), D1((X,)), D1((X,)), D1((X,)),
        D1((2, NP + 1, NCH)), D1((2, NP + 1, NCH)), D1((TPN,)), D1((TPN,)), D1((Y,)), D1((Y,)), D1((4,)),
    ]
    vmem = pl.BlockSpec(memory_space=pltpu.VMEM)
    out = pl.pallas_call(
        functools.partial(mixer, (Z, Y, X, NB, PB, CH)),
        out_shape=jax.ShapeDtypeStruct((Y, PB, D), bf16),
        in_specs=[vmem] * 6,
        out_specs=vmem,
        scratch_shapes=scratch + sems,
        compiler_params=pltpu.CompilerParams(collective_id=0, has_side_effects=True, vmem_limit_bytes=48 * 2**20),
        name="mixer",
    )(normed, w, b, taps, rate, out_gain.reshape(1, DK))
    return jnp.swapaxes(out[:, :NB], 0, 1)


def solution(mesh, sizes=(16, 4, 4)):
    Z, Y, X = sizes
    finer = Mesh(mesh.devices.reshape(Z, Y, X, 2), ("z", "y", "x", "c"))
    return jax.shard_map(
        functools.partial(shards, sizes),
        mesh=finer,
        in_specs=(
            P(SP + TP, None, None), P(), P(SP, TP), P(SP, TP), P(SP, TP), P(SP, TP), P(SP, TP),
            P(None, TP), P(None, TP), P(None, TP), P(TP), P(), P(TP, SP),
        ),
        out_specs=P(SP + TP, None, None),
        check_vma=False,
    )
```

time: 562 us -> 104 us (0.19)
  waiting for transfers between devices: 404 us -> 0 us
  Pallas kernels: 0 us -> 95.7 us
  blocking collectives: 90.7 us -> 0 us
  matrix products: 26.4 us -> 0 us
  between operations: 16.6 us -> 0.79 us
  local copies, waits for them, and re-layouts: 18.4 us -> 6.25 us
    unnamed x8 -> x0, waiting for transfers between devices: 313 us -> none
    pallas_call x0 -> x1, Pallas kernels: none -> 95.7 us  [shards(): pl.pallas_call(functools.partial(mixer, (Z, Y, X, NB, PB, CH)), out_shape...]
    all_gather x8 -> x0, blocking collectives: 90.7 us -> none  [the longest x2 36.2 us: gather_axes(): filled = lax.all_gather(filled, axes[number], axis=dim, tiled=True)]
    all_gather x2 -> x0, waiting for transfers between devices: 90.3 us -> none  [entering(): pieces = jax.tree.map(lambda part: lax.all_gather(part, axis), subtotal)]
    dot_general x61 -> x0, matrix products: 26.4 us -> none  [the longest x21 13.4 us: compose(): jnp.einsum('shde,shev->shdv', second_map, first_shift, precision=highest)]
    unnamed x64 -> x28, local copies, waits for them, and re-layouts: 11.4 us -> 5.41 us
  transfers between devices with their start and end apart: 6 -> 0, of which waited for: 6 -> 0; matrix products, arithmetic and copies ran while one was open for 2% -> 0% of each run, Pallas kernels for 0% -> 0%
where the time goes in v1:
time: 104 us
  Pallas kernels  95.7 us (92%)
  local copies, waits for them, and re-layouts  6.25 us (6%)
  other arithmetic  1.13 us (1%)
    pallas_call x1, Pallas kernels, shards(): pl.pallas_call(functools.partial(mixer, (Z, Y, X, NB, PB, CH)), out_shape...  95.7 us
    unnamed x28, local copies, waits for them, and re-layouts  5.41 us

profile of v1, /device:TPU:1, one launch (start us, length us, event | category | flops | bytes accessed | tf_op | source)
XLA Modules:
  0.0 103.8 jit_solution(10974865686280095164)
XLA Ops:
  0.0 0.0 copy-start.11
  0.0 0.0 copy-start.1
  0.7 0.0 copy-done.11
  0.7 1.0 fusion
  1.8 0.0 copy-start.9
  1.8 0.0 copy-start.10
  1.8 0.1 tile.15
  1.9 0.0 copy-start.8
  1.9 0.6 copy-done.9
  2.4 0.0 copy-done.10
  2.5 0.1 copy-done.8
  2.5 0.0 copy-start.3
  2.5 0.7 copy-done.3
  3.2 0.0 copy-start.4
  3.2 0.7 copy-done.4
  3.9 0.0 copy-start.5
  3.9 0.7 copy-done.5
  4.6 0.0 copy-start.6
  4.6 0.7 copy-done.6
  5.3 0.0 copy-start.7
  5.3 0.7 copy-done.7
  6.0 0.0 copy-start.2
  6.0 0.0 copy-done.1
  6.0 0.7 copy-done.2
  6.7 0.1 fusion.3
  6.8 0.0 copy-start
  6.8 0.6 copy-done
  7.4 95.7 %mixer.1 = bf16[4,16,1024]{2,1,0:T(8,128)(2,1)S(1)} custom-call(bf16[4,16,1024]{2,1,0:T(8,128)(2,1)S(1)} %pad.4.x_ref, bf16[16,640]{1,0:T(8,128)(2,1)S(1)} %constant_dynamic-update-slice_fusion.w_ref, f32[1,128]{1,0:T(1,128)S(1)} %compare_select_fusion.b_ref, f32[4,384]{1,0:T(4,128)S(1)} %maximum_convert_fusion.taps_ref, ...), custom_call_target="tpu_custom_call" | custom-call | tf_op jit(solution)/shard_map/mixer/pallas_call | solution.py:466
  103.1 0.7 copy.15
  (13 shorter events, 0.1 us)
Async XLA Ops:
  0.0 0.7 copy-start.11
  0.0 6.0 %copy-start.1 = (bf16[12,4,1024]{2,1,0:T(4,128)(2,1)S(1)}, bf16[12,4,1024]{2,1,0:T(4,128)(2,1)}, u32[]{:S(2)}) copy-start(bf16[12,4,1024]{2,1,0:T(4,128)(2,1)} %param.13) | copy-start | bytes 294916
  1.8 0.7 copy-start.9
  1.8 0.7 copy-start.10
  1.9 0.7 copy-start.8
  2.5 0.7 copy-start.3
  3.2 0.7 copy-start.4
  3.9 0.7 copy-start.5
  4.6 0.7 copy-start.6
  5.3 0.7 copy-start.7
  6.0 0.7 copy-start.2
  6.8 0.7 copy-start

commit v2 on v1

--- a/solution.py
+++ b/solution.py
@@ -27,6 +27,19 @@
     )
 
 
+PHASES = False
+open_scopes = []
+
+
+def phase(name):
+    if PHASES:
+        while open_scopes:
+            open_scopes.pop().__exit__(None, None, None)
+        if name:
+            open_scopes.append(jax.named_scope(name))
+            open_scopes[-1].__enter__()
+
+
 def dot(a, b):
     return jnp.dot(a.astype(bf16), b.astype(bf16), preferred_element_type=f32)
 
@@ -38,7 +51,8 @@
 
 
 def mixer(
-    dims, x_ref, w_ref, b_ref, taps_ref, rate_ref, gain_ref, out_ref,
+    dims, tok_hbm, ing_hbm, wq_hbm, wk_hbm, wv_hbm, wg_hbm, wo_hbm, wb_hbm, cq_hbm, ck_hbm, cv_hbm, dr_hbm,
+    og_hbm, out_ref, tok, tokf, ing, x_ref, w_ref, b16, b_ref, taps_b, dr, gain_ref, in_s,
     wbuf, bbuf, wbt, xbuf, hin, ext, bext, qs, ks, vs, bs, olo, rdo, mbuf, wo, gsend, grecv, obuf,
     wy_s, wy_r, by_s, by_r, wz_s, wz_r, bz_s, bz_r, xy_s, xy_r, hz_s, hz_r, hy_s, hy_r, hx_s, hx_r,
     hc_s, hc_r, xx_s, xx_r, xc_s, xc_r, ox_s, ox_r, oc_s, oc_r, mz_s, mz_r, g_s, g_r, o_s, o_r, l_s,
@@ -63,13 +77,33 @@
     def zmod(k):
         return lax.rem(z + k + Z, Z)
 
+    phase("barrier")
     barrier = pltpu.get_barrier_semaphore()
     peers = [up, down] + [(z, ymod(k), x, c) for k in range(1, Y)]
     peers += [(z, y, lax.rem(tp + k, TPN) // 2, lax.rem(lax.rem(tp + k, TPN), 2)) for k in range(1, TPN)]
     for peer in peers:
         pl.semaphore_signal(barrier, inc=1, device_id=peer, device_id_type=MESH)
+
+    loads = [(tok_hbm, tok), (ing_hbm, ing), (wb_hbm, b16), (dr_hbm, dr), (og_hbm, gain_ref)]
+    loads += [(ref, w_ref.at[:, i * DK : (i + 1) * DK]) for i, ref in enumerate((wq_hbm, wk_hbm, wv_hbm, wg_hbm, wo_hbm))]
+    loads += [(ref, taps_b.at[i]) for i, ref in enumerate((cq_hbm, ck_hbm, cv_hbm))]
+    loads = [pltpu.make_async_copy(src, dst, in_s.at[i]) for i, (src, dst) in enumerate(loads)]
+    for cp in loads:
+        cp.start()
+    for cp in loads:
+        cp.wait()
+    t = tok[...].astype(f32)
+    t = t * lax.rsqrt(jnp.mean(t * t, axis=-1, keepdims=True) + epsilon)
+    tokf[...] = t * ing[...].reshape(1, 1, D)
+    for s in range(Y):
+        x_ref[s, 0:NB, :] = tokf[:, s, :].astype(bf16)
+    part = lax.rem(z * Y + y, 8)
+    lane = lax.broadcasted_iota(jnp.int32, (1, DK), 1)
+    b = jnp.concatenate([b16[...].astype(f32)] * 8, axis=1)
+    b_ref[...] = jnp.where(lane // ROWS == part, b, 0.0)
     pl.semaphore_wait(barrier, len(peers))
 
+    phase("send_own")
     copies = []
 
     def go(cp):
@@ -103,6 +137,7 @@
     def _():
         copy_to(x_ref, hin, hz_s, hz_r, up).start()
 
+    phase("w_y")
     for k in range(1, Y):
         blk = rows_of(z, ymod(Y - k))
         copy_to(w_ref, wbuf.at[blk], wy_s.at[k], wy_r.at[k], sib).wait_recv()
@@ -118,6 +153,7 @@
     if NM:
         go(copy_to(bbuf.at[z], bbuf.at[z], bz_s.at[1, 1], bz_r.at[1, 1], down))
 
+    phase("tok_y")
     for k in range(1, Y):
         copy_to(x_ref.at[0], xbuf.at[slot0 + ymod(Y - k)], xy_s.at[k], xy_r.at[k], sib).wait_recv()
     local_x.wait()
@@ -149,18 +185,13 @@
             if fminus:
                 copy_to(g, g, bz_s.at[1, k + 1], bz_r.at[1, k + 1], down).start()
 
-    def ring(step):
-        both = max(min(NP - 1, NM - 1), 0)
-        if both:
-
-            @pl.loop(1, both + 1)
-            def _(k):
-                step(k, True, True, True, True)
-
-        for k in range(both + 1, NP + 1):
+    def ring(step, pauses={}):
+        for k in range(1, NP + 1):
             step(k, True, k < NP, k <= NM, k < NM)
-
-    def token_forwards():
+            if k in pauses:
+                pauses[k]()
+
+    def halo_forwards():
         @pl.when(tail_owner)
         def _():
             copy_to(x_ref, hin, hz_s, hz_r, up).wait_recv()
@@ -179,6 +210,7 @@
             for k in range(1, X):
                 copy_to(xbuf.at[HALO], xbuf.at[HALO], hx_s.at[k], hx_r, (z, y, xmod(k), c)).start()
 
+    def token_forwards():
         for k in range(1, X):
             got = pl.ds((xmod(X - k) * 2 + c) * Y, Y)
             copy_to(xbuf.at[got], xbuf.at[got], xx_s.at[k], xx_r.at[k], sib).wait_recv()
@@ -192,10 +224,10 @@
 
             copy_to(xbuf.at[HALO], xbuf.at[HALO], hc_s, hc_r, sib).start()
 
-    w_step_early = min(2, NP - 1)
-    token_forwards()
-    ring(w_step)
-
+    phase("w_ring")
+    ring(w_step, {1: halo_forwards, min(3, NP): token_forwards})
+
+    phase("tok_sib")
     sc = (1 - c)
     for k in range(X):
         got = pl.ds((xmod(X - k) * 2 + sc) * Y, Y)
@@ -207,6 +239,7 @@
 
     local.wait()
 
+    phase("proj")
     PR = TPN * Y * PB
     xs = xbuf[...].reshape(PR + PB, D)
     pre = jnp.dot(xs, wbuf[:, : 4 * DK], preferred_element_type=f32).astype(bf16).astype(f32)
@@ -223,17 +256,20 @@
             ext[8 + to : 8 + to + NB, :] = pre[row : row + NB, :]
             bext[to : to + NB, :] = bpre[row : row + NB, :]
 
+    phase("wo_t")
     for j in range(D // DK):
         tile = wbuf[j * DK : (j + 1) * DK, 4 * DK : 5 * DK].astype(f32)
         wo[tp, :, j * DK : (j + 1) * DK] = tile.T.astype(bf16)
 
+    phase("conv")
+    taps = [taps_b[i].astype(f32) for i in range(3)]
     outs = []
     for kind in range(3):
         lanes = slice(kind * DK, (kind + 1) * DK)
         acc = jnp.zeros((NT, DK), f32)
         for j in range(TAPS):
             at = 8 - (TAPS - 1) + j
-            acc = acc + ext[at : at + NT, lanes] * taps_ref[j : j + 1, lanes]
+            acc = acc + ext[at : at + NT, lanes] * taps[kind][j : j + 1, :]
         outs.append(acc * jax.nn.sigmoid(acc))
     q, k_, v = outs
     qs[...] = q * (lax.rsqrt(jnp.sum(q * q, axis=1, keepdims=True) + epsilon) * DK ** (-0.5))
@@ -246,11 +282,12 @@
         go(copy_to(wo.at[tp], wo.at[tp], ox_s.at[k], ox_r.at[k], (z, y, xmod(k), c)))
     go(copy_to(wo.at[tp], wo.at[tp], oc_s.at[0], oc_r.at[0], sib))
 
-    rate = rate_ref[...]
+    phase("chunks")
+    rate = jnp.broadcast_to(dr[...], (1, DK)) * (1.0 / (NT * Z))
     ri = lax.broadcasted_iota(jnp.int32, (CH, CH), 0)
     ci = lax.broadcasted_iota(jnp.int32, (CH, CH), 1)
     rl = lax.broadcasted_iota(jnp.int32, (CH, DK), 0).astype(f32)
-    rate_c = rate_ref[:, :CH]
+    rate_c = rate[:, :CH]
     decay = jnp.where(ri >= ci, jnp.exp(-rate_c * (ri - ci).astype(f32)), 0.0)
     down_row = jnp.exp(-rate * (rl + 1.0))
     up_row = jnp.exp(-rate * (CH - 1.0 - rl))
@@ -301,6 +338,7 @@
     mbuf[z, :, :DK] = (prefix[:, :DK] - kappa * eye).astype(bf16)
     mbuf[z, :, DK:] = prefix[:, DK:].astype(bf16)
 
+    phase("map_send")
     NCH = mz_s.shape[2]
     PIECE = DK // NCH
 
@@ -346,13 +384,16 @@
             s = far[...]
             far[...] = kappa * s + dot(got[:, :DK], s) + valid * got[:, DK:].astype(f32)
 
+    phase("map_ring")
     ring(m_step)
 
+    phase("wo_fwd")
     for k in range(1, X):
         h = xmod(X - k) * 2 + c
         copy_to(wo.at[h], wo.at[h], ox_s.at[k], ox_r.at[k], sib).wait_recv()
         go(copy_to(wo.at[h], wo.at[h], oc_s.at[k], oc_r.at[k], sib))
 
+    phase("final")
     s = far[...]
     state = jnp.exp(-rate * NT * NP) * s + dot(near_d[...], s) + near_u[...]
     o = olo[...] + dot(rdo[...], state)
@@ -363,6 +404,7 @@
         for t in range(TPN):
             to = (yy * TPN + t) * NB
             gsend[t, yy, 0:NB, :] = olo[to : to + NB, :].astype(bf16)
+    phase("g_send")
     for k in range(1, TPN):
         t = lax.rem(tp + k, TPN)
         go(copy_to(gsend.at[t], grecv.at[tp], g_s.at[k], g_r.at[k], (z, y, t // 2, lax.rem(t, 2))))
@@ -373,17 +415,28 @@
     for k in range(1, TPN):
         t = lax.rem(tp + TPN - k, TPN)
         copy_to(gsend.at[0], grecv.at[t], g_s.at[k], g_r.at[k], sib).wait_recv()
+    phase("out_mm")
     gated = jnp.concatenate([grecv[t].reshape(Y * PB, DK) for t in range(TPN)], axis=1)
     res = jnp.dot(gated, wo[...].reshape(TPN * DK, D), preferred_element_type=f32)
+
+    def put(row, block):
+        for s in range(Y):
+            @pl.when(row == s)
+            def _():
+                tokf[:, s, :] = block[0:NB, :].astype(f32)
+
     obuf[0] = res.astype(bf16).reshape(Y, PB, D)
     for k in range(1, Y):
         go(copy_to(obuf.at[0, ymod(k)], obuf.at[1, y], o_s.at[k], o_r.at[k], (z, ymod(k), x, c)))
-    out_ref[y] = obuf[0, y]
+    put(y, obuf[0, y])
+    phase("o_recv")
     for k in range(1, Y):
         src = ymod(Y - k)
         copy_to(obuf.at[0, 0], obuf.at[1, src], o_s.at[k], o_r.at[k], sib).wait_recv()
-        out_ref[src] = obuf[1, src]
-
+        put(src, obuf[1, src])
+    out_ref[...] = tokf[...].astype(bf16)
+
+    phase("drain")
     for cp in copies:
         cp.wait_send()
     for d, steps in ((0, NP), (1, NM)):
@@ -409,6 +462,7 @@
     @pl.when(c == 1)
     def _():
         copy_to(xbuf.at[HALO], xbuf.at[HALO], hc_s, hc_r, sib).wait_send()
+    phase(None)
 
 
 def shards(
@@ -422,19 +476,20 @@
     NT = Y * TPN * NB
     CH = 128 if NT % 128 == 0 else 96
     NCH = 4
-    values = tokens.astype(f32)
-    scaled = values * lax.rsqrt(jnp.mean(values * values, axis=-1, keepdims=True) + epsilon)
-    normed = jnp.swapaxes((scaled * in_gain).astype(bf16), 0, 1)
-    normed = jnp.pad(normed, ((0, 0), (0, PB - NB), (0, 0)))
-    w = jnp.concatenate([w_query, w_key, w_value, w_gate, w_out.T], axis=1)
-    part = lax.rem(lax.axis_index(SP), 8)
-    lane = lax.broadcasted_iota(jnp.int32, (1, DK), 1)
-    b = jnp.where(lane // ROWS == part, jnp.tile(w_beta.astype(f32).reshape(1, ROWS), (1, 8)), 0.0)
-    taps = jnp.concatenate([conv_query, conv_key, conv_value], axis=1).astype(f32)
-    rate = jnp.broadcast_to((decay_rate / (NT * Z)).reshape(1, 1), (1, DK))
     D1 = pltpu.SemaphoreType.DMA
     NP = Z // 2
     scratch = [
+        pltpu.VMEM((NB, seqs, D), bf16),
+        pltpu.VMEM((NB, seqs, D), f32),
+        pltpu.VMEM((1, D), f32),
+        pltpu.VMEM((seqs, PB, D), bf16),
+        pltpu.VMEM((ROWS, 5 * DK), bf16),
+        pltpu.VMEM((1, ROWS), bf16),
+        pltpu.VMEM((1, DK), f32),
+        pltpu.VMEM((3, TAPS, DK), bf16),
+        pltpu.VMEM((1, 1), f32),
+        pltpu.VMEM((1, DK), f32),
+        D1((13,)),
         pltpu.VMEM((D, 5 * DK), bf16),
         pltpu.VMEM((Z, Y, 1, DK), f32),
         pltpu.VMEM((DK, D), bf16),
@@ -462,17 +517,19 @@
         D1((X,)), D1((X,)), D1((X,)), D1((X,)),
         D1((2, NP + 1, NCH)), D1((2, NP + 1, NCH)), D1((TPN,)), D1((TPN,)), D1((Y,)), D1((Y,)), D1((4,)),
     ]
-    vmem = pl.BlockSpec(memory_space=pltpu.VMEM)
     out = pl.pallas_call(
         functools.partial(mixer, (Z, Y, X, NB, PB, CH)),
-        out_shape=jax.ShapeDtypeStruct((Y, PB, D), bf16),
-        in_specs=[vmem] * 6,
-        out_specs=vmem,
+        out_shape=jax.ShapeDtypeStruct((NB, seqs, D), bf16),
+        in_specs=[pl.BlockSpec(memory_space=pltpu.HBM)] * 13,
+        out_specs=pl.BlockSpec(memory_space=pltpu.VMEM),
         scratch_shapes=scratch + sems,
-        compiler_params=pltpu.CompilerParams(collective_id=0, has_side_effects=True, vmem_limit_bytes=48 * 2**20),
+        compiler_params=pltpu.CompilerParams(collective_id=0, has_side_effects=True),
         name="mixer",
-    )(normed, w, b, taps, rate, out_gain.reshape(1, DK))
-    return jnp.swapaxes(out[:, :NB], 0, 1)
+    )(
+        tokens, in_gain.reshape(1, D), w_query, w_key, w_value, w_gate, w_out.T, w_beta.T,
+        conv_query, conv_key, conv_value, decay_rate.reshape(1, 1), out_gain.reshape(1, DK),
+    )
+    return out
 
 
 def solution(mesh, sizes=(16, 4, 4)):

time: 104 us -> 92.8 us (0.89)
  Pallas kernels: 95.7 us -> 90.4 us
  local copies, waits for them, and re-layouts: 6.25 us -> 1.57 us
  other arithmetic: 1.13 us -> 0 us
    pallas_call x1, Pallas kernels: 95.7 us -> 90.4 us  [shards(): pl.pallas_call(functools.partial(mixer, (Z, Y, X, NB, PB, CH)), out_shape...]
    unnamed x28 -> x1, local copies, waits for them, and re-layouts: 5.41 us -> 1.57 us
where the time goes in v2:
time: 92.8 us; the launch traced here: 92.7 us
  Pallas kernels  90.4 us (97%)
  local copies, waits for them, and re-layouts  1.57 us (2%)
    pallas_call x1, Pallas kernels, shards(): pl.pallas_call(functools.partial(mixer, (Z, Y, X, NB, PB, CH)), out_shape...  90.4 us

profile of v2, /device:TPU:1, one launch (start us, length us, event | category | flops | bytes accessed | tf_op | source)
XLA Modules:
  0.0 92.7 jit_solution(2453358294216536179)
XLA Ops:
  0.7 90.4 %mixer.1 = bf16[12,4,1024]{2,1,0:T(4,128)(2,1)} custom-call(bf16[12,4,1024]{2,1,0:T(4,128)(2,1)} %tok_hbm.1, f32[1,1024]{1,0:T(1,128)} %bitcast.6, bf16[16,128]{1,0:T(8,128)(2,1)} %wq_hbm.1, bf16[16,128]{1,0:T(8,128)(2,1)} %wk_hbm.1, bf16[16,128]{1,0:T(8,128)(2,1)} %wv_hbm.1, bf16[16,128]{1,0:T(8,128)(2,1)} %wg_hbm.1, bf16[16,128]{1,0:T(8,128)(2,1)} %bitcast.7, ...), custom_call_target="tpu_custom_call" | custom-call | tf_op jit(solution)/shard_map/mixer/pallas_call | solution.py:520
  91.1 1.6 %copy.16 = bf16[12,4,1024]{2,1,0:T(4,128)(2,1)} copy(bf16[12,4,1024]{2,1,0:T(4,128)(2,1)} %mixer.1) | data formatting | bytes 196608
